TPU v7x, 512 devices: a whole 4x8x8 slice. The times are simulated.
512 devices in a mesh: sp: 32 (over z, x), tp: 16 (over y, core).
Axes of the slice: x: 4, y: 8, z: 8, core: 2. Of those that a mesh axis runs over, the one named last changes fastest.
Arguments:
- resid: bfloat16 [4096, 2048], P('sp'), may hold values from -6 to 6
- norm_gain: float32 [2048], replicated, may hold values from 0.1 to 1.9
- cotangent: bfloat16 [4096, 2048], P('sp'), may hold values from -6 to 6
- route_ids: int32 [4096, 2], P('sp'), may hold values from 0 to 31, all different within a row; in each aligned block of 128 rows (0 to 127, 128 to 255, ...) at most 12 rows name the same one
- route_weight: float32 [4096, 2], P('sp'), may hold values from 0.25 to 2.25
- expert_gate: bfloat16 [32, 2048, 2048], P('sp', None, 'tp'), may hold values from -0.125 to 0.125
- expert_up: bfloat16 [32, 2048, 2048], P('sp', None, 'tp'), may hold values from -0.125 to 0.125
- expert_down: bfloat16 [32, 2048, 2048], P('sp', 'tp'), may hold values from -0.125 to 0.125
- out_proj: bfloat16 [2048, 4096], P('sp', 'tp'), may hold values from -0.09375 to 0.09375
- mixed: bfloat16 [4096, 4096], P('sp', 'tp'), may hold values from -6 to 6
- query: bfloat16 [4096, 2048], P('sp', 'tp'), may hold values from -6 to 6
- key: bfloat16 [4096, 2048], P('sp', 'tp'), may hold values from -1.5 to 1.5
- value: bfloat16 [4096, 4096], P('sp', 'tp'), may hold values from -6 to 6
- log_decay: float32 [4096, 2048], P('sp', 'tp'), may hold values from -1 to 0, as said below
- span_state: float32 [32, 16, 128, 256], P('sp', 'tp'), may hold values from -24 to 24
Outputs:
- grad_expert_gate: bfloat16 [32, 2048, 2048], P('sp', None, 'tp')
- grad_expert_up: bfloat16 [32, 2048, 2048], P('sp', None, 'tp')
- grad_expert_down: bfloat16 [32, 2048, 2048], P('sp', 'tp')
- grad_out_proj: float32 [2048, 4096], P('sp', 'tp')
- grad_query: bfloat16 [4096, 2048], P('sp', 'tp')
- grad_key: bfloat16 [4096, 2048], P('sp', 'tp')
- grad_value: bfloat16 [4096, 4096], P('sp', 'tp')
- grad_log_decay: float32 [4096, 2048], P('sp', 'tp')
Inputs may be any that keep to these rules, and one draw needn't show every extreme that they name: `route_ids`: A row names 2 different experts. Within each aligned block of 128 rows (the rows of one index of sp) no expert is named by more than 12 rows, and in every draw some expert is named by exactly 12 rows of some block. `log_decay`: every entry is zero or negative.
All inputs are finite; a program needn't handle non-finite values.
Results may differ from a plain program's by a relative error of at most 0.023.
Values may be sent and summed in bfloat16 or wider, within the bound.
No kernel may reach another device: no remote copies, remote signals or barrier semaphores. Data moves between devices by JAX's collectives and lax.ppermute only.
A program may use at most 64 MiB of HBM per device.

v0:
```python
import jax
import jax.numpy as jnp
from jax import lax
from jax.sharding import Mesh
from jax.sharding import PartitionSpec as P

KEY_CHANNELS = 128
DV = 256
TOP = 2
BLOCK = 64
SP = ("z", "x")
TP = ("y", "c")
epsilon = 1e-06


def sum_parts(tiles):
    return jnp.sum(tiles.astype(jnp.float32), axis=0)


def later_sum(states, decays, place):
    count = states.shape[0]
    total = jnp.zeros(states.shape[1:], jnp.float32)
    factor = jnp.ones(decays.shape[1:], jnp.float32)
    for k in range(count):
        later = k > place
        total = total + jnp.where(later, factor, 0.0)[:, None] * states[k].astype(jnp.float32)
        factor = jnp.where(later, factor * decays[k], factor)
    return (total, factor)


def to_all(array, axis):
    count = lax.axis_size(axis)
    copies = jnp.broadcast_to(array[None], (count, *array.shape))
    return lax.all_to_all(copies, axis, 0, 0, tiled=True)


def with_decay(state, decay):
    row = jnp.pad(decay[None, :], ((0, 7), (0, DV - KEY_CHANNELS)))
    return jnp.concatenate([state, row], axis=0).astype(jnp.bfloat16)


def split_decay(filled):
    decays = filled[:, KEY_CHANNELS, :KEY_CHANNELS].astype(jnp.float32)
    return (filled[:, :KEY_CHANNELS], decays)


def into_blocks(values):
    return values.reshape(values.shape[0] // BLOCK, BLOCK, values.shape[1])


def span_forward(query_rows, key_rows, value_rows, grad_rows, decay_rows, entry_state):
    query_blk = into_blocks(query_rows)
    key_blk = into_blocks(key_rows)
    value_blk = into_blocks(value_rows)
    grad_blk = into_blocks(grad_rows)
    cumlog = jnp.cumsum(into_blocks(decay_rows), axis=1)
    block_total = cumlog[:, -1, :]
    to_end = jnp.exp(block_total[:, None, :] - cumlog)
    inner_part = jnp.einsum("nsd,nsj->ndj", key_blk * to_end, value_blk)

    def forward_step(carry_state, step_item):
        piece_part, block_sum = step_item
        return (jnp.exp(block_sum)[:, None] * carry_state + piece_part, carry_state)

    end_state, starts = lax.scan(forward_step, entry_state, (inner_part, block_total))
    own_part = jnp.einsum("ntd,ntj->ndj", query_blk * jnp.exp(cumlog), grad_blk)

    def backward_step(carry_state, step_item):
        piece_part, block_sum = step_item
        return (jnp.exp(block_sum)[:, None] * carry_state + piece_part, carry_state)

    start_cot, after_cot = lax.scan(
        backward_step, jnp.zeros_like(entry_state), (own_part, block_total), reverse=True
    )
    span_total = jnp.sum(block_total, axis=0)
    later_log = span_total[None, :] - jnp.cumsum(block_total, axis=0)
    return ((cumlog, starts, after_cot, later_log, end_state), (jnp.exp(span_total), start_cot))


def span_backward(query_rows, key_rows, value_rows, grad_rows, kept_terms, exit_cot):
    cumlog, starts, after_cot, later_log, end_state = kept_terms
    query_blk = into_blocks(query_rows)
    key_blk = into_blocks(key_rows)
    value_blk = into_blocks(value_rows)
    grad_blk = into_blocks(grad_rows)
    exit_cots = after_cot + jnp.exp(later_log)[:, :, None] * exit_cot
    causal = jnp.arange(BLOCK)[:, None] >= jnp.arange(BLOCK)[None, :]
    decays = jnp.exp(
        jnp.where(causal[None, :, :, None], cumlog[:, :, None, :] - cumlog[:, None, :, :], -jnp.inf)
    )
    scores = jnp.einsum("ntd,nsd,ntsd->nts", query_blk, key_blk, decays)
    grad_scores = jnp.einsum("ntj,nsj->nts", grad_blk, value_blk)
    grad_query = jnp.exp(cumlog) * jnp.einsum("ntj,ndj->ntd", grad_blk, starts)
    grad_query = grad_query + jnp.einsum("nts,nsd,ntsd->ntd", grad_scores, key_blk, decays)
    to_end = jnp.exp(cumlog[:, -1:, :] - cumlog)
    grad_key = jnp.einsum("nts,ntd,ntsd->nsd", grad_scores, query_blk, decays)
    grad_key = grad_key + to_end * jnp.einsum("nsj,ndj->nsd", value_blk, exit_cots)
    grad_value = jnp.einsum("nts,ntj->nsj", scores, grad_blk)
    grad_value = grad_value + jnp.einsum("nsd,ndj->nsj", key_blk * to_end, exit_cots)
    length = query_rows.shape[0]
    key_width = query_rows.shape[1]
    per_position = (query_blk * grad_query - key_blk * grad_key).reshape(length, key_width)
    grad_log = (
        jnp.flip(jnp.cumsum(jnp.flip(per_position, 0), 0), 0)
        + jnp.sum(end_state * exit_cot, axis=1)[None, :]
    )
    return (
        grad_query.reshape(length, key_width),
        grad_key.reshape(length, key_width),
        grad_value.reshape(length, value_rows.shape[1]),
        grad_log,
    )


def on_device(
    resid,
    norm_gain,
    cotangent,
    route_ids,
    route_weight,
    expert_gate,
    expert_up,
    expert_down,
    out_proj,
    mixed,
    query,
    key,
    value,
    log_decay,
    span_state,
):
    tokens_here = resid.shape[0]
    model_width = resid.shape[1]
    half = model_width // 2
    sp_count = lax.axis_size(SP)
    y_count = lax.axis_size("y")
    experts = sp_count * expert_gate.shape[0]
    capacity = 3 * tokens_here // experts
    slots = experts * capacity
    core = lax.axis_index("c")
    resid_f = resid.astype(jnp.float32)
    inverse_rms = lax.rsqrt(jnp.mean(resid_f * resid_f, axis=1, keepdims=True) + epsilon)
    unit_rows = resid_f * inverse_rms
    normed = (unit_rows * norm_gain).astype(jnp.bfloat16)
    pair_expert = route_ids.reshape(-1)
    onehot = (pair_expert[:, None] == jnp.arange(experts, dtype=jnp.int32)[None, :]).astype(
        jnp.int32
    )
    slot_rank = jnp.sum((jnp.cumsum(onehot, axis=0) - onehot) * onehot, axis=1)
    slot_of = (pair_expert * capacity + slot_rank).reshape(tokens_here, TOP)
    slot_a, slot_b = (slot_of[:, 0], slot_of[:, 1])
    packed = lax.broadcasted_iota(jnp.int32, (2 * slots, 2 * tokens_here), 0)
    aim_a = jnp.concatenate([2 * slot_a, 2 * slot_a + 1])[None, :]
    aim_b = jnp.concatenate([2 * slot_b, 2 * slot_b + 1])[None, :]
    hit_a, hit_b = (packed == aim_a, packed == aim_b)
    weight_a = jnp.concatenate([route_weight[:, 0]] * 2)[None, :]
    weight_b = jnp.concatenate([route_weight[:, 1]] * 2)[None, :]
    slot_weight = jnp.sum(
        jnp.where(hit_a, weight_a, 0.0) + jnp.where(hit_b, weight_b, 0.0), axis=1, keepdims=True
    )
    scale = jnp.where(core == 0, 1.0, slot_weight)
    chosen = jnp.where(core == 0, normed, cotangent)
    rows_two = jnp.concatenate([chosen[:, :half], chosen[:, half:]], axis=0)
    sent = jnp.dot(
        (hit_a | hit_b).astype(jnp.bfloat16), rows_two, preferred_element_type=jnp.float32
    )
    sent = (sent * scale).astype(jnp.bfloat16).reshape(sp_count, 2 * capacity, half)
    own = lax.all_to_all(sent, SP, 0, 0, tiled=True).reshape(2 * slots, half)
    other = lax.ppermute(own, "c", [(0, 1), (1, 0)])
    rows_in = jnp.where(core == 0, own, other)
    rows_cot = jnp.where(core == 0, other, own)
    gate_w, up_w, down_w = (expert_gate[0], expert_up[0], expert_down[0])
    width = gate_w.shape[1]
    into_w = jnp.concatenate([gate_w[:half], gate_w[half:], up_w[:half], up_w[half:]], axis=1)
    down_two = jnp.concatenate([down_w[:, :half], down_w[:, half:]], axis=0)
    pre = jnp.dot(rows_in, into_w, preferred_element_type=jnp.float32)
    gate_pre = pre[:, :width] + jnp.roll(pre[:, width : 2 * width], -1, axis=0)
    up_pre = pre[:, 2 * width : 3 * width] + jnp.roll(pre[:, 3 * width :], -1, axis=0)
    hid = lax.dot_general(
        rows_cot, down_two, (((1,), (1,)), ((), ())), preferred_element_type=jnp.float32
    )
    grad_hidden = hid[:, :width] + jnp.roll(hid[:, width:], -1, axis=0)
    gate_sig = jax.nn.sigmoid(gate_pre)
    first = lax.broadcasted_iota(jnp.int32, (2 * slots, 1), 0) % 2 == 0

    def kept(values):
        return jnp.where(first, values, 0.0).astype(jnp.bfloat16)

    hidden = kept(gate_pre * gate_sig * up_pre)
    grad_up_act = kept(grad_hidden * gate_pre * gate_sig)
    grad_gate_act = kept(grad_hidden * up_pre * gate_sig * (1.0 + gate_pre * (1.0 - gate_sig)))
    acts = jnp.concatenate([grad_gate_act, grad_up_act], axis=1)
    pick = (
        lax.broadcasted_iota(jnp.int32, (slots, 2 * slots), 1)
        == 2 * lax.broadcasted_iota(jnp.int32, (slots, 2 * slots), 0)
    ).astype(jnp.bfloat16)
    acts = jnp.dot(pick, acts, preferred_element_type=jnp.float32).astype(jnp.bfloat16)
    out_w = jnp.concatenate([gate_w, up_w], axis=1).reshape(y_count, 2, width, 2 * width)
    out_own = jnp.where(core == 0, out_w[:, 0], out_w[:, 1]).reshape(half, 2 * width)
    out_other = jnp.where(core == 0, out_w[:, 1], out_w[:, 0]).reshape(half, 2 * width)

    def onto(weights):
        return lax.dot_general(
            acts, weights, (((1,), (1,)), ((), ())), preferred_element_type=jnp.float32
        )

    passed = lax.ppermute(onto(out_other).astype(jnp.bfloat16), "c", [(0, 1), (1, 0)])
    pair_sum = (onto(out_own) + passed.astype(jnp.float32)).astype(jnp.bfloat16)
    parts = pair_sum.reshape(slots, y_count, width).transpose(1, 0, 2)
    summed = sum_parts(lax.all_to_all(parts, "y", 0, 0, tiled=True)).astype(jnp.bfloat16)

    def beside(values):
        return jnp.concatenate([values, jnp.roll(values, 1, axis=0)], axis=1)

    grad_in_w = lax.dot_general(
        rows_in,
        jnp.concatenate([beside(grad_gate_act), beside(grad_up_act)], axis=1),
        (((0,), (0,)), ((), ())),
        preferred_element_type=jnp.float32,
    ).astype(jnp.bfloat16)
    grad_gate_w = jnp.concatenate([grad_in_w[:, :width], grad_in_w[:, width : 2 * width]], axis=0)
    grad_up_w = jnp.concatenate(
        [grad_in_w[:, 2 * width : 3 * width], grad_in_w[:, 3 * width :]], axis=0
    )
    grad_out_w = lax.dot_general(
        beside(hidden), rows_cot, (((0,), (0,)), ((), ())), preferred_element_type=jnp.float32
    ).astype(jnp.bfloat16)
    grad_down_w = jnp.concatenate([grad_out_w[:width], grad_out_w[width:]], axis=1)
    out_proj_here, own_tied = lax.optimization_barrier((out_proj, rows_in))
    out_proj_all = to_all(out_proj_here, SP).reshape(model_width, -1)
    returned = lax.all_to_all(
        summed.reshape(experts, capacity, -1), SP, split_axis=0, concat_axis=0, tiled=True
    )
    flat_rows = returned.reshape(slots, -1)
    slot_index = lax.broadcasted_iota(jnp.int32, (slots, tokens_here), 0)
    slot_tokens = ((slot_index == slot_a[None, :]) | (slot_index == slot_b[None, :])).astype(
        jnp.bfloat16
    )
    grad_normed = lax.all_gather(
        lax.dot_general(
            slot_tokens, flat_rows, (((0,), (0,)), ((), ())), preferred_element_type=jnp.float32
        ).astype(jnp.bfloat16),
        ("y", "c"),
        axis=1,
        tiled=True,
    ).astype(jnp.float32)
    scaled = grad_normed * norm_gain
    grad_resid = cotangent.astype(jnp.float32) + inverse_rms * (
        scaled - unit_rows * jnp.mean(scaled * unit_rows, axis=1, keepdims=True)
    )
    grad_resid = grad_resid.astype(jnp.bfloat16)
    grad_mixed = jnp.dot(grad_resid, out_proj_all, preferred_element_type=jnp.float32).astype(
        jnp.bfloat16
    )
    share = lax.dot_general(
        grad_resid, mixed, (((0,), (0,)), ((), ())), preferred_element_type=jnp.float32
    ).astype(jnp.bfloat16)
    grad_out_proj = sum_parts(
        lax.all_to_all(share.reshape(sp_count, model_width // sp_count, -1), SP, 0, 0, tiled=True)
    )
    head_count = query.shape[1] // KEY_CHANNELS
    query_scale = KEY_CHANNELS ** (-0.5)

    def heads_first(values, head_depth):
        return values.reshape(tokens_here, head_count, head_depth).transpose(1, 0, 2)

    query_rows = heads_first(query, KEY_CHANNELS).astype(jnp.float32) * query_scale
    key_rows = heads_first(key, KEY_CHANNELS).astype(jnp.float32)
    value_rows = heads_first(value, DV).astype(jnp.float32)
    grad_rows = heads_first(grad_mixed, DV).astype(jnp.float32)
    decay_rows = heads_first(log_decay, KEY_CHANNELS)
    kept_terms, summary = jax.vmap(span_forward)(
        query_rows, key_rows, value_rows, grad_rows, decay_rows, span_state[0]
    )
    own_decay, own_state = (summary[0][0], summary[1][0])
    near_states, near_decays = split_decay(to_all(with_decay(own_state, own_decay), "x"))
    near_sum, near_factor = later_sum(near_states, near_decays, lax.axis_index("x"))
    group_sum, group_factor = later_sum(near_states, near_decays, -1)
    far_states, far_decays = split_decay(to_all(with_decay(group_sum, group_factor), "z"))
    far_sum, _ = later_sum(far_states, far_decays, lax.axis_index("z"))
    exit_cot = near_sum + near_factor[:, None] * far_sum
    head_grads = jax.vmap(span_backward)(
        query_rows, key_rows, value_rows, grad_rows, kept_terms, exit_cot[None]
    )

    def tokens_first(values):
        return values.transpose(1, 0, 2).reshape(tokens_here, -1)

    grad_query = (tokens_first(head_grads[0]) * query_scale).astype(jnp.bfloat16)
    grad_key = tokens_first(head_grads[1]).astype(jnp.bfloat16)
    grad_value = tokens_first(head_grads[2]).astype(jnp.bfloat16)
    grad_log_decay = tokens_first(head_grads[3])
    return (
        grad_gate_w[None],
        grad_up_w[None],
        grad_down_w[None],
        grad_out_proj,
        grad_query,
        grad_key,
        grad_value,
        grad_log_decay,
    )


def solution(mesh):
    finer = Mesh(mesh.devices.reshape(8, 4, 8, 2), ("z", "x", "y", "c"))
    in_specs = (
        P(SP, None),
        P(),
        P(SP, None),
        P(SP, None),
        P(SP, None),
        P(SP, None, TP),
        P(SP, None, TP),
        P(SP, TP, None),
        P(SP, TP),
        P(SP, TP),
        P(SP, TP),
        P(SP, TP),
        P(SP, TP),
        P(SP, TP),
        P(SP, TP, None, None),
    )
    out_specs = (
        P(SP, None, TP),
        P(SP, None, TP),
        P(SP, TP, None),
        P(SP, TP),
        P(SP, TP),
        P(SP, TP),
        P(SP, TP),
        P(SP, TP),
    )
    return jax.shard_map(
        on_device, mesh=finer, in_specs=in_specs, out_specs=out_specs, check_vma=False
    )
```

profile of v0, /device:TPU:2, one launch (start us, length us, event | category | flops | bytes accessed | tf_op | source)
XLA Modules:
  0.0 222.4 jit_solution(10590077181551964781)
XLA Ops:
  9.0 13.6 %all-to-all-start = ((bf16[32,24,1024]{2,1,0:T(8,128)(2,1)}), bf16[32,24,1024]{2,1,0:T(8,128)(2,1)S(1)}, u32[]{:S(2)}, u32[]{:S(2)}) async-start(bf16[32,24,1024]{2,1,0:T(8,128)(2,1)} %bitcast.383), calls=%async_computation | async-start | bytes 3145728 | tf_op jit(solution)/shard_map/all_to_all | solution.py:168
  25.3 35.7 %all-to-all-done = bf16[32,24,1024]{2,1,0:T(8,128)(2,1)S(1)} async-done(((bf16[32,24,1024]{2,1,0:T(8,128)(2,1)}), bf16[32,24,1024]{2,1,0:T(8,128)(2,1)S(1)}, u32[]{:S(2)}, u32[]{:S(2)}) %all-to-all-start) | async-done | bytes 1572896 | tf_op jit(solution)/shard_map/all_to_all | solution.py:168
  61.0 1.9 collective-permute-start
  63.0 2.3 %broadcast_select_fusion.4 = (bf16[8,1,128,256]{3,2,1,0:T(8,128)(2,1)S(1)}, bf16[8,1,128,256]{3,2,1,0:T(8,128)(2,1)}) fusion(pred[]{:T(512)S(6)} %eq.83, bf16[8,2,128,128]{3,2,1,0:T(8,128)(2,1)S(1)} %bitcast.376, bf16[8,2,128,128]{3,2,1,0:T(8,128)(2,1)} %bitcast.377), kind=kLoop, calls=%fused_computation.94 | loop fusion | flops 3670016 | bytes 2097153 | tf_op jit(solution)/shard_map/jit(_where)/select_n | solution.py:200
  68.2 2.0 fusion.45
  73.5 2.3 %collective-permute-start.1 = (bf16[384,1024]{1,0:T(8,128)(2,1)}, bf16[384,1024]{1,0:T(8,128)(2,1)}, u32[]{:S(2)}, u32[]{:S(2)}) collective-permute-start(bf16[384,1024]{1,0:T(8,128)(2,1)} %convolution_convert_fusion.2), channel_id=1, source_target_pairs={{0,1},{1,0},{2,3},{3,2},{4,5},{5,4},{6,7},{7,6},{8,9},{9,8},{10,11... | collective-permute-start | bytes 2359304 | tf_op jit(solution)/shard_map/ppermute | solution.py:207
  80.7 7.1 %all-to-all-start.1 = ((bf16[8,384,128]{2,1,0:T(8,128)(2,1)}), bf16[8,384,128]{2,1,0:T(8,128)(2,1)S(1)}, u32[]{:S(2)}, u32[]{:S(2)}) async-start(bf16[8,384,128]{2,1,0:T(8,128)(2,1)} %bitcast.374), calls=%async_computation.1 | async-start | bytes 1572864 | tf_op jit(solution)/shard_map/all_to_all | solution.py:210
  87.9 4.4 %fusion.4 = (bf16[2,64,64]{2,1,0:T(8,128)(2,1)}, f32[2,64,128,64]{2,3,1,0:T(8,128)}) fusion(f32[2,128,64]{1,2,0:T(8,128)S(1)} %copy-done.21, f32[2,128,64]{1,2,0:T(8,128)S(1)} %bitcast.384, f32[2,64,128]{2,1,0:T(8,128)S(1)} %bitcast.371, pred[64,64]{1,0:T(8,128)(4,1)S(1)} %iota_compare_fusion.10), kind=kLoop, calls=%fused_computation.11 | loop fusion | flops 5234688 | bytes 4411392 | tf_op jit(solution)/shard_map/vmap(ntd,nsd,ntsd->nts)/dot_general | solution.py:91
  94.3 2.8 %convolution_convert_fusion.3 = bf16[256,1024]{1,0:T(8,128)(2,1)} fusion(bf16[768,1024]{1,0:T(8,128)(2,1)} %collective-permute-done, bf16[768,1024]{1,0:T(8,128)(2,1)S(1)} %bitcast.370, pred[]{:T(512)S(6)} %eq.83, bf16[767,128]{1,0:T(8,128)(2,1)S(1)} %bitcast.395, bf16[1,128]{1,0:T(2,128)(2,1)S(1)} %slice.339, bf16[768,128]{1,0:T(8,128)(2,1)S(1)} %copy-done.22), kind=kOutput, calls=%fused_computation.30 | convolution fusion | flops 404881408 | bytes 4063233 | tf_op jit(solution)/shard_map/dot_general | solution.py:225
  97.1 14.4 %all-to-all-done.1 = bf16[8,384,128]{2,1,0:T(8,128)(2,1)S(1)} async-done(((bf16[8,384,128]{2,1,0:T(8,128)(2,1)}), bf16[8,384,128]{2,1,0:T(8,128)(2,1)S(1)}, u32[]{:S(2)}, u32[]{:S(2)}) %all-to-all-start.1) | async-done | bytes 786464 | tf_op jit(solution)/shard_map/all_to_all | solution.py:210
  112.3 6.5 %all-to-all-start.2 = ((bf16[32,12,128]{2,1,0:T(8,128)(2,1)}), bf16[32,12,128]{2,1,0:T(8,128)(2,1)S(1)}, u32[]{:S(2)}, u32[]{:S(2)}) async-start(bf16[32,12,128]{2,1,0:T(8,128)(2,1)} %reshape.961), calls=%async_computation.2 | async-start | bytes 262144 | tf_op jit(solution)/shard_map/all_to_all | solution.py:231
  118.8 1.9 maximum_bitcast_fusion
  120.7 7.1 %all-to-all-done.2 = bf16[32,12,128]{2,1,0:T(8,128)(2,1)S(1)} async-done(((bf16[32,12,128]{2,1,0:T(8,128)(2,1)}), bf16[32,12,128]{2,1,0:T(8,128)(2,1)S(1)}, u32[]{:S(2)}, u32[]{:S(2)}) %all-to-all-start.2) | async-done | bytes 98336 | tf_op jit(solution)/shard_map/all_to_all | solution.py:231
  129.0 5.6 %all-to-all-start.4 = ((bf16[32,64,256]{2,1,0:T(8,128)(2,1)}), bf16[32,64,256]{2,1,0:T(8,128)(2,1)S(1)}, u32[]{:S(2)}, u32[]{:S(2)}) async-start(bf16[32,64,256]{2,1,0:T(8,128)(2,1)} %broadcast_in_dim.169), calls=%async_computation.4 | async-start | bytes 2097152 | tf_op jit(solution)/shard_map/all_to_all | solution.py:34
  136.7 16.1 %all_gather.3 = bf16[128,2048]{1,0:T(8,128)(2,1)S(1)} all-gather(bf16[128,128]{1,0:T(8,128)(2,1)S(1)} %convolution_convert_fusion.5), channel_id=1, replica_groups=mesh['z'=8,'x'=4,'y'=8,'c'=2] {'y','c'}, dimensions={1}, use_global_device_ids=true | all-gather | bytes 557056 | tf_op jit(solution)/shard_map/all_gather | solution.py:239
  153.6 8.0 %all-to-all-done.4 = bf16[32,64,256]{2,1,0:T(8,128)(2,1)S(1)} async-done(((bf16[32,64,256]{2,1,0:T(8,128)(2,1)}), bf16[32,64,256]{2,1,0:T(8,128)(2,1)S(1)}, u32[]{:S(2)}, u32[]{:S(2)}) %all-to-all-start.4) | async-done | bytes 1048608 | tf_op jit(solution)/shard_map/all_to_all | solution.py:34
  163.5 4.9 %all-to-all-start.5 = ((bf16[4,136,256]{2,1,0:T(8,128)(2,1)}), bf16[4,136,256]{2,1,0:T(8,128)(2,1)S(1)}, u32[]{:S(2)}, u32[]{:S(2)}) async-start(bf16[4,136,256]{2,1,0:T(8,128)(2,1)} %broadcast_in_dim.173), calls=%async_computation.5 | async-start | bytes 557056 | tf_op jit(solution)/shard_map/all_to_all | solution.py:34
  168.7 5.1 %all-to-all-done.5 = bf16[4,136,256]{2,1,0:T(8,128)(2,1)S(1)} async-done(((bf16[4,136,256]{2,1,0:T(8,128)(2,1)}), bf16[4,136,256]{2,1,0:T(8,128)(2,1)S(1)}, u32[]{:S(2)}, u32[]{:S(2)}) %all-to-all-start.5) | async-done | bytes 278560 | tf_op jit(solution)/shard_map/all_to_all | solution.py:34
  174.8 3.5 %all-to-all-start.6 = ((bf16[8,136,256]{2,1,0:T(8,128)(2,1)}), bf16[8,136,256]{2,1,0:T(8,128)(2,1)S(1)}, u32[]{:S(2)}, u32[]{:S(2)}) async-start(bf16[8,136,256]{2,1,0:T(8,128)(2,1)} %broadcast_in_dim.175), calls=%async_computation.6 | async-start | bytes 1114112 | tf_op jit(solution)/shard_map/all_to_all | solution.py:34
  178.4 5.0 %fusion.5 = f32[2,64,128]{2,1,0:T(8,128)S(1)} fusion(f32[2,64,128,64]{2,3,1,0:T(8,128)} %get-tuple-element.289, f32[2,64,128]{2,1,0:T(8,128)S(1)} %copy-done.20, f32[2,64,64]{2,1,0:T(8,128)S(1)} %copy.98), kind=kLoop, calls=%fused_computation.13 | loop fusion | flops 3129344 | bytes 4358144 | tf_op jit(solution)/shard_map/vmap(nts,nsd,ntsd->ntd)/dot_general | solution.py:94
  185.0 2.0 multiply_reduce_fusion
  187.0 6.0 %all-to-all-done.6 = bf16[8,136,256]{2,1,0:T(8,128)(2,1)S(1)} async-done(((bf16[8,136,256]{2,1,0:T(8,128)(2,1)}), bf16[8,136,256]{2,1,0:T(8,128)(2,1)S(1)}, u32[]{:S(2)}, u32[]{:S(2)}) %all-to-all-start.6) | async-done | bytes 557088 | tf_op jit(solution)/shard_map/all_to_all | solution.py:34
  193.0 5.0 %all-to-all-start.3 = ((bf16[32,64,256]{2,1,0:T(8,128)(2,1)}), bf16[32,64,256]{2,1,0:T(8,128)(2,1)S(1)}, u32[]{:S(2)}, u32[]{:S(2)}) async-start(bf16[32,64,256]{2,1,0:T(8,128)(2,1)} %bitcast.28), calls=%async_computation.3 | async-start | bytes 2097152 | tf_op jit(solution)/shard_map/all_to_all | solution.py:259
  201.6 20.1 %all-to-all-done.3 = bf16[32,64,256]{2,1,0:T(8,128)(2,1)S(1)} async-done(((bf16[32,64,256]{2,1,0:T(8,128)(2,1)}), bf16[32,64,256]{2,1,0:T(8,128)(2,1)S(1)}, u32[]{:S(2)}, u32[]{:S(2)}) %all-to-all-start.3) | async-done | bytes 1048608 | tf_op jit(solution)/shard_map/all_to_all | solution.py:259
  (197 shorter events, 39.3 us)
Async XLA Ops:
  0.6 182.9 %copy-start = (bf16[128,256]{1,0:T(8,128)(2,1)S(1)}, bf16[128,256]{1,0:T(8,128)(2,1)}, u32[]{:S(2)}) copy-start(bf16[128,256]{1,0:T(8,128)(2,1)} %param.28) | copy-start | bytes 196612
  9.0 13.6 %copy-start.31 = (f32[128,128]{1,0:T(8,128)S(1)}, f32[128,128]{1,0:T(8,128)}, u32[]{:S(2)}) copy-start(f32[128,128]{1,0:T(8,128)} %param.32) | copy-start | bytes 196612
  9.0 15.6 %copy-start.13 = (bf16[128,256]{1,0:T(8,128)(2,1)S(1)}, bf16[128,256]{1,0:T(8,128)(2,1)}, u32[]{:S(2)}) copy-start(bf16[128,256]{1,0:T(8,128)(2,1)} %param.31) | copy-start | bytes 196612
  9.0 15.6 %copy-start.18 = (bf16[128,128]{1,0:T(8,128)(2,1)S(1)}, bf16[128,128]{1,0:T(8,128)(2,1)}, u32[]{:S(2)}) copy-start(bf16[128,128]{1,0:T(8,128)(2,1)} %param.30) | copy-start | bytes 98308
  9.0 54.0 %copy-start.3 = (bf16[1,2048,128]{2,1,0:T(8,128)(2,1)S(1)}, bf16[1,2048,128]{2,1,0:T(8,128)(2,1)}, u32[]{:S(2)}) copy-start(bf16[1,2048,128]{2,1,0:T(8,128)(2,1)} %param.25) | copy-start | bytes 1572868
  9.0 52.0 %all-to-all-start = ((bf16[32,24,1024]{2,1,0:T(8,128)(2,1)}), bf16[32,24,1024]{2,1,0:T(8,128)(2,1)S(1)}, u32[]{:S(2)}, u32[]{:S(2)}) async-start(bf16[32,24,1024]{2,1,0:T(8,128)(2,1)} %bitcast.383), calls=%async_computation | async-start | bytes 3145728 | tf_op jit(solution)/shard_map/all_to_all | solution.py:168
  22.6 43.2 %copy-start.28 = (bf16[128,128]{1,0:T(8,128)(2,1)S(1)}, bf16[128,128]{1,0:T(8,128)(2,1)}, u32[]{:S(2)}) copy-start(bf16[128,128]{1,0:T(8,128)(2,1)} %param.29) | copy-start | bytes 98308
  61.0 5.7 %collective-permute-start = (bf16[768,1024]{1,0:T(8,128)(2,1)S(1)}, bf16[768,1024]{1,0:T(8,128)(2,1)}, u32[]{:S(2)}, u32[]{:S(2)}) collective-permute-start(bf16[768,1024]{1,0:T(8,128)(2,1)S(1)} %bitcast.368), channel_id=1, source_target_pairs={{0,1},{1,0},{2,3},{3,2},{4,5},{5,4},{6,7},{7,6},{8,9},{9,8},{10,11... | collective-permute-start | bytes 4718600 | tf_op jit(solution)/shard_map/ppermute | solution.py:169
  65.9 21.9 %copy-start.11 = (f32[128,128]{1,0:T(8,128)}, f32[128,128]{1,0:T(8,128)S(1)}, u32[]{:S(2)}) copy-start(f32[128,128]{1,0:T(8,128)S(1)} %convert_multiply_fusion.18) | copy-start | bytes 196612
  73.5 4.5 %collective-permute-start.1 = (bf16[384,1024]{1,0:T(8,128)(2,1)}, bf16[384,1024]{1,0:T(8,128)(2,1)}, u32[]{:S(2)}, u32[]{:S(2)}) collective-permute-start(bf16[384,1024]{1,0:T(8,128)(2,1)} %convolution_convert_fusion.2), channel_id=1, source_target_pairs={{0,1},{1,0},{2,3},{3,2},{4,5},{5,4},{6,7},{7,6},{8,9},{9,8},{10,11... | collective-permute-start | bytes 2359304 | tf_op jit(solution)/shard_map/ppermute | solution.py:207
  80.7 30.8 %all-to-all-start.1 = ((bf16[8,384,128]{2,1,0:T(8,128)(2,1)}), bf16[8,384,128]{2,1,0:T(8,128)(2,1)S(1)}, u32[]{:S(2)}, u32[]{:S(2)}) async-start(bf16[8,384,128]{2,1,0:T(8,128)(2,1)} %bitcast.374), calls=%async_computation.1 | async-start | bytes 1572864 | tf_op jit(solution)/shard_map/all_to_all | solution.py:210
  97.1 30.7 %copy-start.32 = (bf16[64,256]{1,0:T(8,128)(2,1)S(1)}, bf16[64,256]{1,0:T(8,128)(2,1)}, u32[]{:S(2)}) copy-start(bf16[64,256]{1,0:T(8,128)(2,1)} %param.27) | copy-start | bytes 98308
  112.3 15.5 %all-to-all-start.2 = ((bf16[32,12,128]{2,1,0:T(8,128)(2,1)}), bf16[32,12,128]{2,1,0:T(8,128)(2,1)S(1)}, u32[]{:S(2)}, u32[]{:S(2)}) async-start(bf16[32,12,128]{2,1,0:T(8,128)(2,1)} %reshape.961), calls=%async_computation.2 | async-start | bytes 262144 | tf_op jit(solution)/shard_map/all_to_all | solution.py:231
  120.7 13.9 %copy-start.10 = (bf16[1024,128]{1,0:T(8,128)(2,1)S(1)}, bf16[1024,128]{1,0:T(8,128)(2,1)}, u32[]{:S(2)}) copy-start(bf16[1024,128]{1,0:T(8,128)(2,1)} %get-tuple-element.275) | copy-start | bytes 786436
  129.0 32.6 %all-to-all-start.4 = ((bf16[32,64,256]{2,1,0:T(8,128)(2,1)}), bf16[32,64,256]{2,1,0:T(8,128)(2,1)S(1)}, u32[]{:S(2)}, u32[]{:S(2)}) async-start(bf16[32,64,256]{2,1,0:T(8,128)(2,1)} %broadcast_in_dim.169), calls=%async_computation.4 | async-start | bytes 2097152 | tf_op jit(solution)/shard_map/all_to_all | solution.py:34
  135.5 17.3 %copy-start.30 = (f32[2048]{0:T(1024)S(1)}, f32[2048]{0:T(1024)}, u32[]{:S(2)}) copy-start(f32[2048]{0:T(1024)} %param.20) | copy-start | bytes 24580
  135.5 17.3 %copy-start.34 = (f32[128]{0:T(128)S(1)}, f32[128]{0:T(128)}, u32[]{:S(2)}) copy-start(f32[128]{0:T(128)} %copy-done.33) | copy-start | bytes 1540
  135.5 17.6 %copy-start.7 = (bf16[128,2048]{1,0:T(8,128)(2,1)S(1)}, bf16[128,2048]{1,0:T(8,128)(2,1)}, u32[]{:S(2)}) copy-start(bf16[128,2048]{1,0:T(8,128)(2,1)} %param.21) | copy-start | bytes 1572868
  163.5 14.8 %copy-start.20 = (f32[2,64,128]{2,1,0:T(8,128)S(1)}, f32[2,64,128]{2,1,0:T(8,128)}, u32[]{:S(2)}) copy-start(f32[2,64,128]{2,1,0:T(8,128)} %get-tuple-element.297) | copy-start | bytes 196612
  163.5 10.2 %all-to-all-start.5 = ((bf16[4,136,256]{2,1,0:T(8,128)(2,1)}), bf16[4,136,256]{2,1,0:T(8,128)(2,1)S(1)}, u32[]{:S(2)}, u32[]{:S(2)}) async-start(bf16[4,136,256]{2,1,0:T(8,128)(2,1)} %broadcast_in_dim.173), calls=%async_computation.5 | async-start | bytes 557056 | tf_op jit(solution)/shard_map/all_to_all | solution.py:34
  174.8 18.2 %all-to-all-start.6 = ((bf16[8,136,256]{2,1,0:T(8,128)(2,1)}), bf16[8,136,256]{2,1,0:T(8,128)(2,1)S(1)}, u32[]{:S(2)}, u32[]{:S(2)}) async-start(bf16[8,136,256]{2,1,0:T(8,128)(2,1)} %broadcast_in_dim.175), calls=%async_computation.6 | async-start | bytes 1114112 | tf_op jit(solution)/shard_map/all_to_all | solution.py:34
  187.0 11.4 %copy-start.19 = (bf16[128,128]{1,0:T(8,128)(2,1)S(1)}, bf16[128,128]{1,0:T(8,128)(2,1)}, u32[]{:S(2)}) copy-start(bf16[128,128]{1,0:T(8,128)(2,1)} %param.30) | copy-start | bytes 98308
  187.0 11.4 %copy-start.29 = (bf16[128,128]{1,0:T(8,128)(2,1)S(1)}, bf16[128,128]{1,0:T(8,128)(2,1)}, u32[]{:S(2)}) copy-start(bf16[128,128]{1,0:T(8,128)(2,1)} %param.29) | copy-start | bytes 98308
  193.0 28.6 %all-to-all-start.3 = ((bf16[32,64,256]{2,1,0:T(8,128)(2,1)}), bf16[32,64,256]{2,1,0:T(8,128)(2,1)S(1)}, u32[]{:S(2)}, u32[]{:S(2)}) async-start(bf16[32,64,256]{2,1,0:T(8,128)(2,1)} %bitcast.28), calls=%async_computation.3 | async-start | bytes 2097152 | tf_op jit(solution)/shard_map/all_to_all | solution.py:259
  (26 other events, 107.8 us)
where the time goes:
time: 224 us; the launch traced here: 222 us
  waiting for transfers between devices  97 us (43%)
  starting transfers between devices  50.6 us (23%)
  other arithmetic  29.2 us (13%)
  matrix products  16.6 us (7%)
  blocking collectives  16.1 us (7%)
  local copies, waits for them, and re-layouts  11.3 us (5%)
    all_to_all x1, waiting for transfers between devices, on_device(): own = lax.all_to_all(sent, SP, 0, 0, tiled=True).reshape(2 * slots, half)  35.7 us
    all_to_all x1, waiting for transfers between devices, on_device(): lax.all_to_all(share.reshape(sp_count, model_width // sp_count, -1), SP,...  20.1 us
    all_to_all x3, waiting for transfers between devices, to_all(): return lax.all_to_all(copies, axis, 0, 0, tiled=True)  19.1 us
    all_gather x1, blocking collectives, on_device(): lax.all_gather(lax.dot_general(slot_tokens, flat_rows, (((0,), (0,)), (()...  16.1 us
    all_to_all x1, waiting for transfers between devices, on_device(): lax.all_to_all(parts, 'y', 0, 0, tiled=True)  14.4 us
    all_to_all x3, starting transfers between devices, to_all(): return lax.all_to_all(copies, axis, 0, 0, tiled=True)  14.1 us
    all_to_all x1, starting transfers between devices, on_device(): own = lax.all_to_all(sent, SP, 0, 0, tiled=True).reshape(2 * slots, half)  13.6 us
    all_to_all x1, waiting for transfers between devices, on_device(): lax.all_to_all(summed.reshape(experts, capacity, -1), SP, split_axis=0, c...  7.14 us
  transfers between devices with their start and end apart: 9, of which 8 were waited for; matrix products, arithmetic and copies ran while one was open for 15% of the time, Pallas kernels for 0%

commit v1 on v0

--- a/solution.py
+++ b/solution.py
@@ -11,6 +11,11 @@
 SP = ("z", "x")
 TP = ("y", "c")
 epsilon = 1e-06
+
+
+def all_by_exchange(block, name, dim):
+    sent = jnp.stack([block] * lax.axis_size(name))
+    return jnp.concatenate(lax.all_to_all(sent, name, 0, 0), axis=dim)
 
 
 def sum_parts(tiles):
@@ -236,13 +241,12 @@
     slot_tokens = ((slot_index == slot_a[None, :]) | (slot_index == slot_b[None, :])).astype(
         jnp.bfloat16
     )
-    grad_normed = lax.all_gather(
+    grad_normed = all_by_exchange(
         lax.dot_general(
             slot_tokens, flat_rows, (((0,), (0,)), ((), ())), preferred_element_type=jnp.float32
         ).astype(jnp.bfloat16),
         ("y", "c"),
-        axis=1,
-        tiled=True,
+        1,
     ).astype(jnp.float32)
     scaled = grad_normed * norm_gain
     grad_resid = cotangent.astype(jnp.float32) + inverse_rms * (

time: 224 us -> 254 us (1.13)
  blocking collectives: 16.1 us -> 52.7 us
  starting transfers between devices: 50.6 us -> 40.7 us
  local copies, waits for them, and re-layouts: 11.3 us -> 14.2 us
  matrix products: 16.6 us -> 13.8 us
    all_to_all x0 -> x1, blocking collectives: none -> 52.7 us  [on_device(): own = lax.all_to_all(sent, SP, 0, 0, tiled=True).reshape(2 * slots, half)]
    all_to_all x1, waiting for transfers between devices: 35.7 us -> 8.24 us  [all_by_exchange(): return jnp.concatenate(lax.all_to_all(sent, name, 0, 0), axis=dim)]
    all_gather x1 -> x0, blocking collectives: 16.1 us -> none  [on_device(): lax.all_gather(lax.dot_general(slot_tokens, flat_rows, (((0,), (0,)), (()...]
    all_to_all x3, waiting for transfers between devices: 19.1 us -> 34.8 us  [to_all(): return lax.all_to_all(copies, axis, 0, 0, tiled=True)]
    all_to_all x1, starting transfers between devices: 13.6 us -> 3.57 us  [all_by_exchange(): return jnp.concatenate(lax.all_to_all(sent, name, 0, 0), axis=dim)]
    all_to_all x1, waiting for transfers between devices: 14.4 us -> 22.8 us  [on_device(): lax.all_to_all(parts, 'y', 0, 0, tiled=True)]
    all_to_all x1, waiting for transfers between devices: 20.1 us -> 24 us  [on_device(): lax.all_to_all(share.reshape(sp_count, model_width // sp_count, -1), SP,...]
  transfers between devices with their start and end apart: 9 -> 9, of which waited for: 8 -> 8; matrix products, arithmetic and copies ran while one was open for 15% -> 14% of each run, Pallas kernels for 0% -> 0%
where the time goes in v1:
time: 254 us; the launch traced here: 252 us
  waiting for transfers between devices  98.9 us (39%)
  blocking collectives  52.7 us (21%)
  starting transfers between devices  40.7 us (16%)
  other arithmetic  30.1 us (12%)
  local copies, waits for them, and re-layouts  14.2 us (6%)
  matrix products  13.8 us (5%)
    all_to_all x1, blocking collectives, on_device(): own = lax.all_to_all(sent, SP, 0, 0, tiled=True).reshape(2 * slots, half)  52.7 us
    all_to_all x3, waiting for transfers between devices, to_all(): return lax.all_to_all(copies, axis, 0, 0, tiled=True)  34.8 us
    all_to_all x1, waiting for transfers between devices, on_device(): lax.all_to_all(share.reshape(sp_count, model_width // sp_count, -1), SP,...  24 us
    all_to_all x1, waiting for transfers between devices, on_device(): lax.all_to_all(parts, 'y', 0, 0, tiled=True)  22.8 us
    all_to_all x3, starting transfers between devices, to_all(): return lax.all_to_all(copies, axis, 0, 0, tiled=True)  15.2 us
    all_to_all x1, waiting for transfers between devices, on_device(): lax.all_to_all(summed.reshape(experts, capacity, -1), SP, split_axis=0, c...  8.42 us
    all_to_all x1, waiting for transfers between devices, all_by_exchange(): return jnp.concatenate(lax.all_to_all(sent, name, 0, 0), axis=dim)  8.24 us
    all_to_all x1, starting transfers between devices, on_device(): lax.all_to_all(parts, 'y', 0, 0, tiled=True)  7.09 us
  transfers between devices with their start and end apart: 9, of which 8 were waited for; matrix products, arithmetic and copies ran while one was open for 14% of the time, Pallas kernels for 0%

profile of v1, /device:TPU:2, one launch (start us, length us, event | category | flops | bytes accessed | tf_op | source)
XLA Modules:
  0.0 252.2 jit_solution(4890277538563998212)
XLA Ops:
  7.7 52.7 %all_to_all.40 = bf16[32,24,1024]{2,1,0:T(8,128)(2,1)S(1)} all-to-all(bf16[32,24,1024]{2,1,0:T(8,128)(2,1)S(1)} %bitcast.390), channel_id=1, replica_groups=mesh['z'=8,'x'=4,'y'=8,'c'=2] {'z','x'}, dimensions={0} | all-to-all | bytes 3145728 | tf_op jit(solution)/shard_map/all_to_all | solution.py:173
  60.4 1.9 collective-permute-start
  62.8 1.9 broadcast_select_fusion.4
  67.3 2.0 fusion.45
  71.4 2.3 collective-permute-start.1
  77.2 7.1 %all-to-all-start.1 = ((bf16[8,384,128]{2,1,0:T(8,128)(2,1)}), bf16[8,384,128]{2,1,0:T(8,128)(2,1)}, u32[]{:S(2)}, u32[]{:S(2)}) async-start(bf16[8,384,128]{2,1,0:T(8,128)(2,1)} %bitcast.381), calls=%async_computation.1 | async-start | bytes 1572864 | tf_op jit(solution)/shard_map/all_to_all | solution.py:215
  85.2 22.8 %all-to-all-done.1 = bf16[8,384,128]{2,1,0:T(8,128)(2,1)} async-done(((bf16[8,384,128]{2,1,0:T(8,128)(2,1)}), bf16[8,384,128]{2,1,0:T(8,128)(2,1)}, u32[]{:S(2)}, u32[]{:S(2)}) %all-to-all-start.1) | async-done | bytes 786464 | tf_op jit(solution)/shard_map/all_to_all | solution.py:215
  110.0 5.6 %all-to-all-start.2 = ((bf16[32,12,128]{2,1,0:T(8,128)(2,1)}), bf16[32,12,128]{2,1,0:T(8,128)(2,1)S(1)}, u32[]{:S(2)}, u32[]{:S(2)}) async-start(bf16[32,12,128]{2,1,0:T(8,128)(2,1)} %reshape.967), calls=%async_computation.2 | async-start | bytes 262144 | tf_op jit(solution)/shard_map/all_to_all | solution.py:236
  116.1 8.4 %all-to-all-done.2 = bf16[32,12,128]{2,1,0:T(8,128)(2,1)S(1)} async-done(((bf16[32,12,128]{2,1,0:T(8,128)(2,1)}), bf16[32,12,128]{2,1,0:T(8,128)(2,1)S(1)}, u32[]{:S(2)}, u32[]{:S(2)}) %all-to-all-start.2) | async-done | bytes 98336 | tf_op jit(solution)/shard_map/all_to_all | solution.py:236
  125.7 3.6 %all-to-all-start.3 = ((bf16[16,128,128]{2,1,0:T(8,128)(2,1)}), bf16[16,128,128]{2,1,0:T(8,128)(2,1)S(1)}, u32[]{:S(2)}, u32[]{:S(2)}) async-start(bf16[16,128,128]{2,1,0:T(8,128)(2,1)} %stack.2), calls=%async_computation.3 | async-start | bytes 1048576 | tf_op jit(solution)/shard_map/all_to_all | solution.py:18
  129.4 5.4 %fusion.4 = (bf16[2,64,64]{2,1,0:T(8,128)(2,1)}, f32[2,64,128,64]{2,3,1,0:T(8,128)}) fusion(f32[2,128,64]{1,2,0:T(8,128)} %get-tuple-element.306, f32[2,128,64]{1,2,0:T(8,128)} %bitcast.391, f32[2,64,128]{2,1,0:T(8,128)S(1)} %bitcast.379, pred[64,64]{1,0:T(8,128)(4,1)S(1)} %iota_compare_fusion.10), kind=kLoop, calls=%fused_computation.11 | loop fusion | flops 5234688 | bytes 4411392 | tf_op jit(solution)/shard_map/vmap(ntd,nsd,ntsd->nts)/dot_general | solution.py:96
  137.0 8.2 %all-to-all-done.3 = bf16[16,128,128]{2,1,0:T(8,128)(2,1)S(1)} async-done(((bf16[16,128,128]{2,1,0:T(8,128)(2,1)}), bf16[16,128,128]{2,1,0:T(8,128)(2,1)S(1)}, u32[]{:S(2)}, u32[]{:S(2)}) %all-to-all-start.3) | async-done | bytes 524320 | tf_op jit(solution)/shard_map/all_to_all | solution.py:18
  147.1 6.2 %all-to-all-start.5 = ((bf16[32,64,256]{2,1,0:T(8,128)(2,1)}), bf16[32,64,256]{2,1,0:T(8,128)(2,1)}, u32[]{:S(2)}, u32[]{:S(2)}) async-start(bf16[32,64,256]{2,1,0:T(8,128)(2,1)} %broadcast_in_dim.169), calls=%async_computation.5 | async-start | bytes 2097152 | tf_op jit(solution)/shard_map/all_to_all | solution.py:39
  153.3 1.9 maximum_bitcast_fusion
  157.7 2.0 convolution_convert_fusion.3
  161.8 20.1 %all-to-all-done.5 = bf16[32,64,256]{2,1,0:T(8,128)(2,1)} async-done(((bf16[32,64,256]{2,1,0:T(8,128)(2,1)}), bf16[32,64,256]{2,1,0:T(8,128)(2,1)}, u32[]{:S(2)}, u32[]{:S(2)}) %all-to-all-start.5) | async-done | bytes 1048608 | tf_op jit(solution)/shard_map/all_to_all | solution.py:39
  185.1 5.5 %all-to-all-start.6 = ((bf16[4,136,256]{2,1,0:T(8,128)(2,1)}), bf16[4,136,256]{2,1,0:T(8,128)(2,1)S(1)}, u32[]{:S(2)}, u32[]{:S(2)}) async-start(bf16[4,136,256]{2,1,0:T(8,128)(2,1)} %broadcast_in_dim.173), calls=%async_computation.6 | async-start | bytes 557056 | tf_op jit(solution)/shard_map/all_to_all | solution.py:39
  190.9 5.6 %all-to-all-done.6 = bf16[4,136,256]{2,1,0:T(8,128)(2,1)S(1)} async-done(((bf16[4,136,256]{2,1,0:T(8,128)(2,1)}), bf16[4,136,256]{2,1,0:T(8,128)(2,1)S(1)}, u32[]{:S(2)}, u32[]{:S(2)}) %all-to-all-start.6) | async-done | bytes 278560 | tf_op jit(solution)/shard_map/all_to_all | solution.py:39
  197.5 3.5 %all-to-all-start.7 = ((bf16[8,136,256]{2,1,0:T(8,128)(2,1)}), bf16[8,136,256]{2,1,0:T(8,128)(2,1)S(1)}, u32[]{:S(2)}, u32[]{:S(2)}) async-start(bf16[8,136,256]{2,1,0:T(8,128)(2,1)} %broadcast_in_dim.175), calls=%async_computation.7 | async-start | bytes 1114112 | tf_op jit(solution)/shard_map/all_to_all | solution.py:39
  201.1 5.0 %fusion.5 = f32[2,64,128]{2,1,0:T(8,128)S(1)} fusion(f32[2,64,128,64]{2,3,1,0:T(8,128)} %get-tuple-element.299, f32[2,64,128]{2,1,0:T(8,128)S(1)} %copy-done.14, f32[2,64,64]{2,1,0:T(8,128)S(1)} %copy.127), kind=kLoop, calls=%fused_computation.13 | loop fusion | flops 3129344 | bytes 4358144 | tf_op jit(solution)/shard_map/vmap(nts,nsd,ntsd->ntd)/dot_general | solution.py:99
  207.7 1.9 multiply_reduce_fusion
  209.7 9.1 %all-to-all-done.7 = bf16[8,136,256]{2,1,0:T(8,128)(2,1)S(1)} async-done(((bf16[8,136,256]{2,1,0:T(8,128)(2,1)}), bf16[8,136,256]{2,1,0:T(8,128)(2,1)S(1)}, u32[]{:S(2)}, u32[]{:S(2)}) %all-to-all-start.7) | async-done | bytes 557088 | tf_op jit(solution)/shard_map/all_to_all | solution.py:39
  218.8 5.0 %all-to-all-start.4 = ((bf16[32,64,256]{2,1,0:T(8,128)(2,1)}), bf16[32,64,256]{2,1,0:T(8,128)(2,1)S(1)}, u32[]{:S(2)}, u32[]{:S(2)}) async-start(bf16[32,64,256]{2,1,0:T(8,128)(2,1)} %bitcast.30), calls=%async_computation.4 | async-start | bytes 2097152 | tf_op jit(solution)/shard_map/all_to_all | solution.py:263
  227.4 24.0 %all-to-all-done.4 = bf16[32,64,256]{2,1,0:T(8,128)(2,1)S(1)} async-done(((bf16[32,64,256]{2,1,0:T(8,128)(2,1)}), bf16[32,64,256]{2,1,0:T(8,128)(2,1)S(1)}, u32[]{:S(2)}, u32[]{:S(2)}) %all-to-all-start.4) | async-done | bytes 1048608 | tf_op jit(solution)/shard_map/all_to_all | solution.py:263
  (185 shorter events, 39.2 us)
Async XLA Ops:
  0.6 205.6 %copy-start = (bf16[128,256]{1,0:T(8,128)(2,1)S(1)}, bf16[128,256]{1,0:T(8,128)(2,1)}, u32[]{:S(2)}) copy-start(bf16[128,256]{1,0:T(8,128)(2,1)} %param.28) | copy-start | bytes 196612
  7.6 54.7 %copy-start.24 = (f32[128,128]{1,0:T(8,128)S(1)}, f32[128,128]{1,0:T(8,128)}, u32[]{:S(2)}) copy-start(f32[128,128]{1,0:T(8,128)} %param.32) | copy-start | bytes 196612
  7.6 54.8 %copy-start.7 = (bf16[128,256]{1,0:T(8,128)(2,1)S(1)}, bf16[128,256]{1,0:T(8,128)(2,1)}, u32[]{:S(2)}) copy-start(bf16[128,256]{1,0:T(8,128)(2,1)} %param.31) | copy-start | bytes 196612
  7.7 54.8 %copy-start.12 = (bf16[128,128]{1,0:T(8,128)(2,1)S(1)}, bf16[128,128]{1,0:T(8,128)(2,1)}, u32[]{:S(2)}) copy-start(bf16[128,128]{1,0:T(8,128)(2,1)} %param.30) | copy-start | bytes 98308
  60.4 5.5 %collective-permute-start = (bf16[768,1024]{1,0:T(8,128)(2,1)S(1)}, bf16[768,1024]{1,0:T(8,128)(2,1)}, u32[]{:S(2)}, u32[]{:S(2)}) collective-permute-start(bf16[768,1024]{1,0:T(8,128)(2,1)S(1)} %bitcast.376), channel_id=1, source_target_pairs={{0,1},{1,0},{2,3},{3,2},{4,5},{5,4},{6,7},{7,6},{8,9},{9,8},{10,11... | collective-permute-start | bytes 4718600 | tf_op jit(solution)/shard_map/ppermute | solution.py:174
  71.4 4.2 %collective-permute-start.1 = (bf16[384,1024]{1,0:T(8,128)(2,1)S(1)}, bf16[384,1024]{1,0:T(8,128)(2,1)S(1)}, u32[]{:S(2)}, u32[]{:S(2)}) collective-permute-start(bf16[384,1024]{1,0:T(8,128)(2,1)S(1)} %convolution_convert_fusion.2), channel_id=1, source_target_pairs={{0,1},{1,0},{2,3},{3,2},{4,5},{5,4},{6,7},{7,6},{8,9},{9,8},{10,11... | collective-permute-start | bytes 2359304 | tf_op jit(solution)/shard_map/ppermute | solution.py:212
  76.1 8.9 %copy-start.1 = (f32[1,1,128,256]{3,2,1,0:T(8,128)S(1)}, f32[1,1,128,256]{3,2,1,0:T(8,128)}, u32[]{:S(2)}) copy-start(f32[1,1,128,256]{3,2,1,0:T(8,128)} %param.33) | copy-start | bytes 393220
  77.2 30.9 %all-to-all-start.1 = ((bf16[8,384,128]{2,1,0:T(8,128)(2,1)}), bf16[8,384,128]{2,1,0:T(8,128)(2,1)}, u32[]{:S(2)}, u32[]{:S(2)}) async-start(bf16[8,384,128]{2,1,0:T(8,128)(2,1)} %bitcast.381), calls=%async_computation.1 | async-start | bytes 1572864 | tf_op jit(solution)/shard_map/all_to_all | solution.py:215
  85.2 40.5 %copy-start.9 = (bf16[2,1,128,256]{3,2,1,0:T(8,128)(2,1)}, bf16[2,1,128,256]{3,2,1,0:T(8,128)(2,1)S(1)}, u32[]{:S(2)}) copy-start(bf16[2,1,128,256]{3,2,1,0:T(8,128)(2,1)S(1)} %get-tuple-element.142) | copy-start | bytes 393220
  85.2 40.5 %copy-start.30 = (f32[2,1,128]{2,1,0:T(1,128)}, f32[2,1,128]{2,1,0:T(1,128)S(1)}, u32[]{:S(2)}) copy-start(f32[2,1,128]{2,1,0:T(1,128)S(1)} %get-tuple-element.450) | copy-start | bytes 3076
  110.0 14.6 %all-to-all-start.2 = ((bf16[32,12,128]{2,1,0:T(8,128)(2,1)}), bf16[32,12,128]{2,1,0:T(8,128)(2,1)S(1)}, u32[]{:S(2)}, u32[]{:S(2)}) async-start(bf16[32,12,128]{2,1,0:T(8,128)(2,1)} %reshape.967), calls=%async_computation.2 | async-start | bytes 262144 | tf_op jit(solution)/shard_map/all_to_all | solution.py:236
  125.7 19.5 %all-to-all-start.3 = ((bf16[16,128,128]{2,1,0:T(8,128)(2,1)}), bf16[16,128,128]{2,1,0:T(8,128)(2,1)S(1)}, u32[]{:S(2)}, u32[]{:S(2)}) async-start(bf16[16,128,128]{2,1,0:T(8,128)(2,1)} %stack.2), calls=%async_computation.3 | async-start | bytes 1048576 | tf_op jit(solution)/shard_map/all_to_all | solution.py:18
  147.1 34.7 %all-to-all-start.5 = ((bf16[32,64,256]{2,1,0:T(8,128)(2,1)}), bf16[32,64,256]{2,1,0:T(8,128)(2,1)}, u32[]{:S(2)}, u32[]{:S(2)}) async-start(bf16[32,64,256]{2,1,0:T(8,128)(2,1)} %broadcast_in_dim.169), calls=%async_computation.5 | async-start | bytes 2097152 | tf_op jit(solution)/shard_map/all_to_all | solution.py:39
  161.3 22.1 %copy-start.6 = (f32[128,128]{1,0:T(8,128)S(1)}, f32[128,128]{1,0:T(8,128)}, u32[]{:S(2)}) copy-start(f32[128,128]{1,0:T(8,128)} %convert_multiply_fusion.17) | copy-start | bytes 196612
  161.8 21.9 %copy-start.31 = (f32[2,1,128]{2,1,0:T(1,128)S(1)}, f32[2,1,128]{2,1,0:T(1,128)}, u32[]{:S(2)}) copy-start(f32[2,1,128]{2,1,0:T(1,128)} %copy-done.30) | copy-start | bytes 3076
  183.7 6.9 %copy-start.8 = (bf16[128,256]{1,0:T(8,128)(2,1)S(1)}, bf16[128,256]{1,0:T(8,128)(2,1)}, u32[]{:S(2)}) copy-start(bf16[128,256]{1,0:T(8,128)(2,1)} %param.31) | copy-start | bytes 196612
  185.1 15.9 %copy-start.14 = (f32[2,64,128]{2,1,0:T(8,128)S(1)}, f32[2,64,128]{2,1,0:T(8,128)}, u32[]{:S(2)}) copy-start(f32[2,64,128]{2,1,0:T(8,128)} %get-tuple-element.307) | copy-start | bytes 196612
  185.1 11.4 %all-to-all-start.6 = ((bf16[4,136,256]{2,1,0:T(8,128)(2,1)}), bf16[4,136,256]{2,1,0:T(8,128)(2,1)S(1)}, u32[]{:S(2)}, u32[]{:S(2)}) async-start(bf16[4,136,256]{2,1,0:T(8,128)(2,1)} %broadcast_in_dim.173), calls=%async_computation.6 | async-start | bytes 557056 | tf_op jit(solution)/shard_map/all_to_all | solution.py:39
  197.5 21.3 %all-to-all-start.7 = ((bf16[8,136,256]{2,1,0:T(8,128)(2,1)}), bf16[8,136,256]{2,1,0:T(8,128)(2,1)S(1)}, u32[]{:S(2)}, u32[]{:S(2)}) async-start(bf16[8,136,256]{2,1,0:T(8,128)(2,1)} %broadcast_in_dim.175), calls=%async_computation.7 | async-start | bytes 1114112 | tf_op jit(solution)/shard_map/all_to_all | solution.py:39
  209.6 14.6 %copy-start.13 = (bf16[128,128]{1,0:T(8,128)(2,1)S(1)}, bf16[128,128]{1,0:T(8,128)(2,1)}, u32[]{:S(2)}) copy-start(bf16[128,128]{1,0:T(8,128)(2,1)} %param.30) | copy-start | bytes 98308
  209.6 14.6 %copy-start.22 = (bf16[128,128]{1,0:T(8,128)(2,1)S(1)}, bf16[128,128]{1,0:T(8,128)(2,1)}, u32[]{:S(2)}) copy-start(bf16[128,128]{1,0:T(8,128)(2,1)} %param.29) | copy-start | bytes 98308
  209.7 14.6 %copy-start.26 = (f32[1,2,1,128]{3,2,1,0:T(1,128)S(1)}, f32[1,2,1,128]{3,2,1,0:T(1,128)}, u32[]{:S(2)}) copy-start(f32[1,2,1,128]{3,2,1,0:T(1,128)} %copy-done.25) | copy-start | bytes 3076
  209.7 14.6 %copy-start.27 = (f32[2,128]{1,0:T(2,128)S(1)}, f32[2,128]{1,0:T(2,128)}, u32[]{:S(2)}) copy-start(f32[2,128]{1,0:T(2,128)} %subtract_exponential_fusion.1) | copy-start | bytes 3076
  218.8 32.6 %all-to-all-start.4 = ((bf16[32,64,256]{2,1,0:T(8,128)(2,1)}), bf16[32,64,256]{2,1,0:T(8,128)(2,1)S(1)}, u32[]{:S(2)}, u32[]{:S(2)}) async-start(bf16[32,64,256]{2,1,0:T(8,128)(2,1)} %bitcast.30), calls=%async_computation.4 | async-start | bytes 2097152 | tf_op jit(solution)/shard_map/all_to_all | solution.py:263
  (18 other events, 66.6 us)
